TPU v7x, 128 devices: a whole 4x4x4 slice. The times are simulated.
128 devices in a mesh: sp: 64 (over z, y, x), tp: 2 (over core).
Axes of the slice: x: 4, y: 4, z: 4, core: 2. Of those that a mesh axis runs over, the one named last changes fastest.
Arguments:
- projected_queries: bfloat16 [32768, 1024], P('sp', 'tp'), may hold values from -6 to 6
- projected_keys: bfloat16 [32768, 1024], P('sp', 'tp'), may hold values from -6 to 6
- projected_values: bfloat16 [32768, 1024], P('sp', 'tp'), may hold values from -6 to 6
- output_gate_values: bfloat16 [32768, 1024], P('sp', 'tp'), may hold values from -6 to 6
- write_strength_logits: bfloat16 [32768, 8], P('sp', 'tp'), may hold values from -6.5 to 3
- decay_input_logits: bfloat16 [32768, 8], P('sp', 'tp'), may hold values from -5 to 5
- head_rate_logarithm: float32 [8], P('tp'), may hold values from -8 to 2.3
- extra_log_decay: float32 [32768, 8], P('sp', 'tp'), may hold values from -0.7 to 0
- per_head_norm_gain: float32 [128], replicated, may hold values from 0.1 to 1.9
- output_matrix: bfloat16 [1024, 2048], replicated, may hold values from -0.1875 to 0.1875
- residual: bfloat16 [32768, 2048], P(('sp', 'tp')), may hold values from -6 to 6
- mixture_norm_gain: float32 [2048], replicated, may hold values from 0.1 to 1.9
- selected_expert_index: int32 [32768, 4], P(('sp', 'tp')), may hold values from 0 to 127, all different within a row; in each aligned block of 256 rows (0 to 255, 256 to 511, ...) at most 12 rows name the same one
- routing_weight: float32 [32768, 4], P(('sp', 'tp')), may hold values from 0.1 to 0.9
- routed_gate_weight: bfloat16 [128, 2048, 512], P(('sp', 'tp')), may hold values from -0.125 to 0.125
- routed_up_weight: bfloat16 [128, 2048, 512], P(('sp', 'tp')), may hold values from -0.125 to 0.125
- routed_down_weight: bfloat16 [128, 512, 2048], P(('sp', 'tp')), may hold values from -0.25 to 0.25
- common_gate_weight: bfloat16 [2048, 512], replicated, may hold values from -0.125 to 0.125
- common_up_weight: bfloat16 [2048, 512], replicated, may hold values from -0.125 to 0.125
- common_down_weight: bfloat16 [512, 2048], replicated, may hold values from -0.25 to 0.25
Outputs:
- block_out: bfloat16 [32768, 2048], P(('sp', 'tp'))
Inputs may be any that keep to these rules, and one draw needn't show every extreme that they name: `selected_expert_index`: each row names 4 different experts. Among the rows that one device holds, no expert is named more than 12 times.
All inputs are finite; a program needn't handle non-finite values.
Results may differ from a plain program's by a relative error of at most 0.008.
Values may be sent and summed in bfloat16 or wider, within the bound.
No kernel may reach another device: no remote copies, remote signals or barrier semaphores. Data moves between devices by JAX's collectives and lax.ppermute only.
A program may use at most 192 MiB of HBM per device.

v0:
```python
import jax
import jax.numpy as jnp
from jax import lax
from jax.sharding import Mesh
from jax.sharding import PartitionSpec as P

TOP_K = 4
SPAN = 64
SP = ("sp_0", "sp_1", "sp_2")
SP_TP = ("sp_0", "sp_1", "sp_2", "tp")


EPS = 1e-06
HIGH = lax.Precision.HIGHEST


def nothing_yet(shard, identity):
    return jax.tree.map(
        lambda a, e: jnp.broadcast_to(jnp.asarray(e, a.dtype), a.shape), shard, identity
    )


def entering(shard, axes, combine, identity):
    before = start = nothing_yet(shard, identity)
    running = shard
    for axis in reversed(axes):
        count, mine = (lax.axis_size(axis), lax.axis_index(axis))
        pieces = jax.tree.map(lambda part: lax.all_gather(part, axis), running)
        inside, running = (start, start)
        for k in range(count):
            passed = k < mine
            running = combine(running, jax.tree.map(lambda part: part[k], pieces))
            inside = jax.tree.map(lambda new, old: jnp.where(passed, new, old), running, inside)
        before = combine(inside, before)
    return before


def items_in_groups(shard, axis, split_dim, concat_dim, work, item_dim, out_dim):
    items = jax.tree.leaves(shard)[0].shape[item_dim]
    count = 2 if items % 2 == 0 else 1
    gathered = []
    for k in range(count):
        group = jax.tree.map(
            lambda a: lax.slice_in_dim(
                a, k * (items // count), (k + 1) * (items // count), axis=item_dim
            ),
            shard,
        )
        gathered.append(
            work(
                lax.all_to_all(
                    group, axis, split_axis=split_dim, concat_axis=concat_dim, tiled=True
                )
            )
        )
    return jax.tree.map(lambda *parts: jnp.concatenate(parts, axis=out_dim), *gathered)


def unit_heads(raw, heads):
    active = jax.nn.silu(raw.astype(jnp.float32)).reshape(raw.shape[0], heads, -1)
    return active * lax.rsqrt(jnp.sum(active * active, axis=-1, keepdims=True) + EPS)


def prepare_inputs(
    projected_queries,
    projected_keys,
    projected_values,
    write_strength_logits,
    decay_input_logits,
    head_rate_logarithm,
    extra_log_decay,
):
    heads = head_rate_logarithm.shape[0]
    queries = unit_heads(projected_queries, heads)
    keys = unit_heads(projected_keys, heads)
    values = jax.nn.silu(projected_values.astype(jnp.float32)).reshape(
        projected_values.shape[0], heads, -1
    )
    beta = jax.nn.sigmoid(write_strength_logits.astype(jnp.float32))
    decay_logarithm = extra_log_decay - jnp.exp(head_rate_logarithm)[None, :] * jax.nn.softplus(
        decay_input_logits.astype(jnp.float32) - 6.0
    )
    return (queries, keys, values, beta, decay_logarithm)


def block_terms(queries, keys, values, beta, decay_logarithm):
    length, heads, width = queries.shape
    number = length // SPAN

    def split(array):
        return jnp.moveaxis(array.reshape(number, SPAN, heads, -1), 2, 0)

    q_blocks = split(queries)
    k_blocks = split(keys)
    v_blocks = split(values)
    b_blocks = split(beta[..., None])[..., 0]
    g_cumul = jnp.cumsum(split(decay_logarithm[..., None])[..., 0], axis=-1)
    place = jnp.arange(SPAN)
    causal = place[:, None] >= place[None, :]
    strict = place[:, None] > place[None, :]
    spread = jnp.where(causal, g_cumul[..., :, None] - g_cumul[..., None, :], 0.0)
    decay = jnp.where(causal, jnp.exp(spread), 0.0)
    k_beta = k_blocks * b_blocks[..., None]
    inner = jnp.einsum("hncd,hnsd->hncs", k_beta, k_blocks, precision=HIGH)
    lower = jnp.where(strict, inner * decay, 0.0) + jnp.eye(SPAN, dtype=jnp.float32)
    right = jnp.concatenate(
        [v_blocks * b_blocks[..., None], k_beta * jnp.exp(g_cumul)[..., None]], axis=-1
    )
    solved = jax.scipy.linalg.solve_triangular(lower, right, lower=True, unit_diagonal=True)
    u_part = solved[..., :width]
    w_part = solved[..., width:]
    scores = jnp.einsum("hncd,hnsd->hncs", q_blocks, k_blocks, precision=HIGH) * decay
    q_decayed = q_blocks * jnp.exp(g_cumul)[..., None]
    log_last = g_cumul[..., -1]
    k_decayed = k_blocks * jnp.exp(log_last[..., None] - g_cumul)[..., None]
    return (q_decayed, scores, u_part, w_part, k_decayed, log_last)


def run_blocks(terms, start):

    def advance(state, items):
        q_one, s_one, u_one, w_one, k_one, log_one = items
        fresh = u_one - jnp.einsum("hcd,hde->hce", w_one, state, precision=HIGH)
        result = jnp.einsum("hcd,hde->hce", q_one, state, precision=HIGH)
        result = result + jnp.einsum("hcs,hse->hce", s_one, fresh, precision=HIGH)
        state = state * jnp.exp(log_one)[:, None, None] + jnp.einsum(
            "hcd,hce->hde", k_one, fresh, precision=HIGH
        )
        return (state, result)

    items = tuple((jnp.moveaxis(array, 1, 0) for array in terms))
    _, results = lax.scan(advance, start, items)
    number, heads, span, width = results.shape
    return results.transpose(0, 2, 1, 3).reshape(number * span, heads, width)


def state_maps(terms):
    q_decayed, scores, u_part, w_part, k_decayed, log_last = terms
    heads, number, span, width = u_part.shape
    identity = jnp.broadcast_to(jnp.eye(width, dtype=jnp.float32), (heads, width, width))
    empty = jnp.zeros((heads, width, width), jnp.float32)

    def compose(pair, items):
        mapping, carried = pair
        w_one, u_one, k_one, log_one = items
        factor = jnp.exp(log_one)[:, None, None]
        erased = jnp.einsum("hcd,hde->hce", w_one, mapping, precision=HIGH)
        mapping = mapping * factor - jnp.einsum("hcd,hce->hde", k_one, erased, precision=HIGH)
        fresh = u_one - jnp.einsum("hcd,hde->hce", w_one, carried, precision=HIGH)
        carried = carried * factor + jnp.einsum("hcd,hce->hde", k_one, fresh, precision=HIGH)
        return ((mapping, carried), None)

    items = tuple((jnp.moveaxis(array, 1, 0) for array in (w_part, u_part, k_decayed, log_last)))
    (mapping, carried), _ = lax.scan(compose, (identity, empty), items)
    return (mapping, carried, identity, empty)


def chain(earlier, later):
    mapping = jnp.einsum("hij,hjk->hik", later[0], earlier[0], precision=HIGH)
    carried = jnp.einsum("hij,hjk->hik", later[0], earlier[1], precision=HIGH) + later[1]
    return (mapping, carried)


def finish(head_mix, output_gate_values, per_head_norm_gain):
    length, heads, width = head_mix.shape
    scaled = head_mix * lax.rsqrt(jnp.mean(head_mix * head_mix, axis=-1, keepdims=True) + EPS)
    gated = (
        scaled
        * per_head_norm_gain
        * jax.nn.silu(output_gate_values.astype(jnp.float32).reshape(length, heads, width))
    )
    return gated.reshape(length, heads * width).astype(jnp.bfloat16)


def normalize(stream, gain):
    wide = stream.astype(jnp.float32)
    return (wide * lax.rsqrt(jnp.mean(wide * wide, axis=-1, keepdims=True) + EPS) * gain).astype(
        jnp.bfloat16
    )


def feed_forward(rows, w_gate, w_up, w_down):
    hidden = jax.nn.silu(jnp.dot(rows, w_gate, preferred_element_type=jnp.float32))
    hidden = (hidden * jnp.dot(rows, w_up, preferred_element_type=jnp.float32)).astype(jnp.bfloat16)
    return jnp.dot(hidden, w_down, preferred_element_type=jnp.float32)


def shards(
    projected_queries,
    projected_keys,
    projected_values,
    output_gate_values,
    write_strength_logits,
    decay_input_logits,
    head_rate_logarithm,
    extra_log_decay,
    per_head_norm_gain,
    output_matrix,
    residual,
    mixture_norm_gain,
    selected_expert_index,
    routing_weight,
    routed_gate_weight,
    routed_up_weight,
    routed_down_weight,
    common_gate_weight,
    common_up_weight,
    common_down_weight,
):
    prepared_inputs = prepare_inputs(
        projected_queries,
        projected_keys,
        projected_values,
        write_strength_logits,
        decay_input_logits,
        head_rate_logarithm,
        extra_log_decay,
    )
    terms = block_terms(*prepared_inputs)
    mapping, carried, identity, empty = state_maps(terms)
    before = entering((mapping, carried), SP, chain, (identity, empty))
    heads_out = finish(run_blocks(terms, before[1]), output_gate_values, per_head_norm_gain)
    token_heads = lax.all_to_all(heads_out, "tp", split_axis=0, concat_axis=1, tiled=True)
    projected = jnp.dot(token_heads, output_matrix, preferred_element_type=jnp.float32)
    attended = (residual.astype(jnp.float32) + projected).astype(jnp.bfloat16)
    normed = normalize(attended, mixture_norm_gain)
    length = normed.shape[0]
    experts = lax.axis_size(SP) * lax.axis_size("tp")
    room = max(2, length * TOP_K * 3 // (2 * experts))
    flat_ids = selected_expert_index.reshape(-1)
    total = flat_ids.shape[0]
    onehot = (flat_ids[:, None] == jnp.arange(experts, dtype=jnp.int32)[None, :]).astype(
        jnp.bfloat16
    )
    place = jnp.arange(total, dtype=jnp.int32)
    earlier = (place[:, None] > place[None, :]).astype(jnp.bfloat16)
    before_count = jnp.dot(earlier, onehot, preferred_element_type=jnp.float32)
    slot = jnp.sum(before_count * onehot.astype(jnp.float32), axis=1).astype(jnp.int32)
    target = flat_ids * room + slot
    source = jnp.zeros((experts * room,), jnp.int32).at[target].set(place // TOP_K)
    filled = jnp.zeros((experts * room,), jnp.bool_).at[target].set(True)
    outgoing = jnp.where(filled[:, None], normed[source], jnp.zeros((), jnp.bfloat16)).reshape(
        experts, room, -1
    )

    def expert_ffn(arrived):
        flat = arrived.reshape(-1, arrived.shape[-1])
        result = feed_forward(
            flat, routed_gate_weight[0], routed_up_weight[0], routed_down_weight[0]
        ).astype(jnp.bfloat16)
        return result.reshape(arrived.shape)

    def serve(arrived):
        return lax.all_to_all(expert_ffn(arrived), SP_TP, split_axis=0, concat_axis=0, tiled=True)

    back = items_in_groups(outgoing, SP_TP, 0, 0, serve, 1, 1)
    returned_rows = back.reshape(experts * room, -1)[target].reshape(length, TOP_K, -1)
    routed = jnp.einsum("rk,rkd->rd", routing_weight, returned_rows.astype(jnp.float32))
    shared = feed_forward(normed, common_gate_weight, common_up_weight, common_down_weight)
    return (attended.astype(jnp.float32) + shared + routed).astype(jnp.bfloat16)


def solution(mesh):
    finer = Mesh(mesh.devices.reshape(4, 4, 4, mesh.shape["tp"]), ("sp_0", "sp_1", "sp_2", "tp"))
    in_specs = (
        P(SP, "tp"),
        P(SP, "tp"),
        P(SP, "tp"),
        P(SP, "tp"),
        P(SP, "tp"),
        P(SP, "tp"),
        P("tp"),
        P(SP, "tp"),
        P(),
        P(),
        P(SP_TP, None),
        P(),
        P(SP_TP, None),
        P(SP_TP, None),
        P(SP_TP, None, None),
        P(SP_TP, None, None),
        P(SP_TP, None, None),
        P(),
        P(),
        P(),
    )
    out_specs = P(SP_TP, None)
    return jax.shard_map(
        shards, mesh=finer, in_specs=in_specs, out_specs=out_specs, check_vma=False
    )
```

profile of v0, /device:TPU:1, one launch (start us, length us, event | category | flops | bytes accessed | tf_op | source)
XLA Modules:
  0.0 804.6 jit_solution(5793430192315798224)
XLA Ops:
  9.5 2.7 fusion.188
  12.2 2.6 mul.218
  14.8 1.9 reduce_sum.45
  16.8 2.5 reshape.170
  19.5 5.1 fusion.76
  24.7 158.7 %custom-call.4 = f32[4,8,1,64,64]{3,4,2,1,0:T(8,128)} custom-call(f32[4,8,1,64,64]{4,3,2,1,0:T(8,128)} %fusion.76), custom_call_target="InvertDiagBlocksLowerTriangular" | custom-call | tf_op jit(solution)/shard_map/jit(_solve_triangular)/vmap(vmap())/triangular_solve | solution.py:109
  184.6 2.5 reshape_reshape.3
  187.1 2.3 bitcast_multiply_fusion.2
  189.4 2.0 fusion.40
  195.7 45.6 %while.26 = (s32[]{:T(128)}, f32[4,128,128]{2,1,0:T(8,128)S(1)}, f32[4,128,128]{2,1,0:T(8,128)S(1)}, f32[8,4]{1,0:T(8,128)S(1)}, f32[8,4,64,128]{3,2,1,0:T(8,128...) while((s32[]{:T(128)}, f32[4,128,128]{2,1,0:T(8,128)S(1)}, ...), condition=%wide.region_3.4_spmd.clone, body=%wide.region_2.3_spmd.clone.sunk | while | flops 201752576 | bytes 2755244 | solution.py:154
  199.8 1.5 convolution_subtract_fusion.7
  205.5 1.5 convolution_subtract_fusion.7
  211.2 1.5 convolution_subtract_fusion.7
  216.9 1.5 convolution_subtract_fusion.7
  222.6 1.5 convolution_subtract_fusion.7
  228.3 1.5 convolution_subtract_fusion.7
  234.1 1.5 convolution_subtract_fusion.7
  239.8 1.5 convolution_subtract_fusion.7
  243.1 24.3 %all-gather.13.cloned.1.call-done = f32[16,128,128]{2,1,0:T(8,128)} async-done(((f32[4,128,128]{2,1,0:T(8,128)}), f32[16,128,128]{2,1,0:T(8,128)}) %all-gather.13.cloned.1.call-update) | async-done | bytes 1048592 | tf_op jit(solution)/shard_map/all_gather | solution.py:28
  267.4 26.1 %all-gather.19.cloned.1.call-done = f32[16,128,128]{2,1,0:T(8,128)} async-done(((f32[4,128,128]{2,1,0:T(8,128)}), f32[16,128,128]{2,1,0:T(8,128)}) %all-gather.19.cloned.1.call-update) | async-done | bytes 1048592 | tf_op jit(solution)/shard_map/all_gather | solution.py:28
  304.6 4.3 scatter_custom_fusion.1
  308.9 1.7 fusion.189
  310.6 13.5 %all-gather.21.cloned.1.call-done = f32[16,128,128]{2,1,0:T(8,128)} async-done(((f32[4,128,128]{2,1,0:T(8,128)}), f32[16,128,128]{2,1,0:T(8,128)}) %all-gather.21.cloned.1.call-update) | async-done | bytes 1048592 | tf_op jit(solution)/shard_map/all_gather | solution.py:28
  324.1 26.0 %all-gather.15.cloned.1.call-done = f32[16,128,128]{2,1,0:T(8,128)} async-done(((f32[4,128,128]{2,1,0:T(8,128)}), f32[16,128,128]{2,1,0:T(8,128)}) %all-gather.15.cloned.1.call-update) | async-done | bytes 1048592 | tf_op jit(solution)/shard_map/all_gather | solution.py:28
  356.5 2.6 mul.233
  359.1 2.6 reduce_sum.46
  361.6 2.6 reshape.171
  365.3 2.9 multiply_bitcast_fusion
  372.8 4.8 scatter_custom_fusion
  377.7 4.5 fusion.63
  382.3 2.0 bitcast_multiply_fusion.1
  387.1 19.9 %all-gather.17.cloned.1.call-done = f32[16,128,128]{2,1,0:T(8,128)} async-done(((f32[4,128,128]{2,1,0:T(8,128)}), f32[16,128,128]{2,1,0:T(8,128)}) %all-gather.17.cloned.1.call-update) | async-done | bytes 1048592 | tf_op jit(solution)/shard_map/all_gather | solution.py:28
  413.8 48.5 %while.25 = (s32[]{:T(128)}, f32[4,128,128]{2,1,0:T(8,128)S(1)}, f32[8,4,64,128]{3,2,1,0:T(8,128)S(1)}, f32[8,4]{1,0:T(8,128)}, f32[8,4,64,128]{3,2,1,0:T(8,128)...) while((s32[]{:T(128)}, f32[4,128,128]{2,1,0:T(8,128)S(1)}, ...), condition=%wide.region_6.7_spmd, body=%wide.region_5.6_spmd.sunk | while | flops 176357376 | bytes 2754721 | solution.py:132
  430.5 1.5 convolution_add_fusion.19
  436.5 1.5 convolution_add_fusion.19
  460.7 1.5 convolution_add_fusion.19
  464.7 6.7 all_to_all.39
  471.4 3.9 fusion.37
  476.6 7.1 gather_fusion
  483.7 10.6 %gather.9 = bf16[128,12,2048]{2,1,0:T(8,128)(2,1)} reshape(bf16[1536,2048]{1,0:T(8,128)(2,1)} %gather_fusion) | data formatting | bytes 12582912 | tf_op jit(solution)/shard_map/gather | solution.py:242
  494.3 7.4 broadcast_select_fusion
  501.7 7.1 fusion.190
  508.8 61.0 %all_to_all.40 = bf16[128,6,2048]{2,1,0:T(8,128)(2,1)} all-to-all(bf16[128,6,2048]{2,1,0:T(8,128)(2,1)S(1)} %get-tuple-element.229), channel_id=1, replica_groups=mesh['sp_0'=4,'sp_1'=4,'sp_2'=4,'tp'=2] {'sp_0','sp_1','sp_2','tp'}, dimensions={0} | all-to-all | bytes 6291456 | tf_op jit(solution)/shard_map/all_to_all | solution.py:51
  569.9 5.5 all-to-all-start.3
  575.4 6.4 reshape.173
  581.8 5.5 fusion.52
  587.3 8.1 %convolution_convert_fusion.1 = bf16[768,2048]{1,0:T(8,128)(2,1)} fusion(bf16[1,512,2048]{2,1,0:T(8,128)(2,1)S(1)} %copy-done, f32[768,512]{1,0:T(8,128)} %fusion.52, bf16[768,2048]{1,0:T(8,128)(2,1)} %reshape.173, bf16[1,2048,512]{2,1,0:T(8,128)(2,1)} %param.39), kind=kOutput, calls=%fused_computation.52 | convolution fusion | flops 3225157632 | bytes 12058624 | tf_op jit(solution)/shard_map/dot_general | solution.py:185
  595.4 6.3 reshape.174
  601.7 26.4 %all-to-all-done.3 = bf16[128,6,2048]{2,1,0:T(8,128)(2,1)} async-done(((bf16[128,6,2048]{2,1,0:T(8,128)(2,1)}), bf16[128,6,2048]{2,1,0:T(8,128)(2,1)}, u32[]{:S(2)}, u32[]{:S(2)}) %all-to-all-start.3) | async-done | bytes 3145760 | tf_op jit(solution)/shard_map/all_to_all | solution.py:51
  628.1 5.5 all-to-all-start.2
  633.6 6.4 reshape.175
  640.0 5.5 fusion.50
  645.5 8.1 %convolution_convert_fusion = bf16[768,2048]{1,0:T(8,128)(2,1)} fusion(bf16[1,512,2048]{2,1,0:T(8,128)(2,1)S(1)} %copy-done, f32[768,512]{1,0:T(8,128)} %fusion.50, bf16[768,2048]{1,0:T(8,128)(2,1)} %reshape.175, bf16[1,2048,512]{2,1,0:T(8,128)(2,1)} %param.39), kind=kOutput, calls=%fused_computation.51 | convolution fusion | flops 3225157632 | bytes 12058624 | tf_op jit(solution)/shard_map/dot_general | solution.py:185
  653.7 6.3 reshape.176
  659.9 26.4 %all-to-all-done.2 = bf16[128,6,2048]{2,1,0:T(8,128)(2,1)} async-done(((bf16[128,6,2048]{2,1,0:T(8,128)(2,1)}), bf16[128,6,2048]{2,1,0:T(8,128)(2,1)}, u32[]{:S(2)}, u32[]{:S(2)}) %all-to-all-start.2) | async-done | bytes 3145760 | tf_op jit(solution)/shard_map/all_to_all | solution.py:254
  686.4 5.9 all-to-all-start.4
  692.5 3.2 fusion.193
  695.6 49.2 %all-to-all-done.4 = bf16[128,6,2048]{2,1,0:T(8,128)(2,1)} async-done(((bf16[128,6,2048]{2,1,0:T(8,128)(2,1)}), bf16[128,6,2048]{2,1,0:T(8,128)(2,1)}, u32[]{:S(2)}, u32[]{:S(2)}) %all-to-all-start.4) | async-done | bytes 3145760 | tf_op jit(solution)/shard_map/all_to_all | solution.py:254
  744.8 10.5 %pad_maximum_fusion = bf16[128,12,2048]{2,1,0:T(8,128)(2,1)} fusion(bf16[128,6,2048]{2,1,0:T(8,128)(2,1)} %all-to-all-done.4, bf16[128,6,2048]{2,1,0:T(8,128)(2,1)} %all-to-all-done.2), kind=kLoop, calls=%fused_computation.47 | loop fusion | flops 12582912 | bytes 12582912 | tf_op jit(solution)/shard_map/concatenate | solution.py:56
  755.4 10.7 %reshape.177 = bf16[1536,2048]{1,0:T(8,128)(2,1)} reshape(bf16[128,12,2048]{2,1,0:T(8,128)(2,1)} %pad_maximum_fusion) | data formatting | bytes 12582912 | tf_op jit(solution)/shard_map/reshape | solution.py:257
  766.1 12.4 %gather_fusion.1 = bf16[1024,2048]{1,0:T(8,128)(2,1)} fusion(bf16[1536,2048]{1,0:T(8,128)(2,1)} %reshape.177, s32[1024]{0:T(1024)S(1)} %broadcast_clamp_fusion), kind=kCustom, calls=%fused_computation.1 | custom fusion | bytes 8392704 | tf_op jit(solution)/shard_map/gather | solution.py:257
  778.5 7.2 reshape.178
  785.7 5.8 fusion.196
  791.6 5.8 fusion.35
  (276 shorter events, 122.8 us)
Async XLA Ops:
  6.5 580.7 %copy-start = (bf16[1,512,2048]{2,1,0:T(8,128)(2,1)S(1)}, bf16[1,512,2048]{2,1,0:T(8,128)(2,1)}, u32[]{:S(2)}) copy-start(bf16[1,512,2048]{2,1,0:T(8,128)(2,1)} %param.40) | copy-start | bytes 6291460
  6.5 260.9 %all-gather.13.cloned.1.call-start = ((), (), s32[]{:S(2)}) async-start(), calls=%async_computation.5 | async-start | bytes 1310720 | tf_op jit(solution)/shard_map/all_gather | solution.py:28
  14.8 4.7 copy-start.50
  19.5 163.8 %copy-start.45 = (bf16[512,512]{1,0:T(8,128)(2,1)S(1)}, bf16[512,512]{1,0:T(8,128)(2,1)}, u32[]{:S(2)}) copy-start(bf16[512,512]{1,0:T(8,128)(2,1)} %param.26) | copy-start | bytes 1572868
  187.1 2.3 copy-start.37
  191.7 2.1 copy-start.5
  241.3 0.7 copy-start.1
  241.3 0.8 copy-start.2
  241.3 26.1 %copy-start.52 = (f32[8,4]{1,0:T(8,128)}, f32[8,4]{1,0:T(8,128)S(1)}, u32[]{:S(2)}) copy-start(f32[8,4]{1,0:T(8,128)S(1)} %get-tuple-element.435) | copy-start | bytes 388
  242.1 51.5 %all-gather.19.cloned.1.call-start = ((), (), s32[]{:S(2)}) async-start(), calls=%async_computation.8 | async-start | bytes 1310720 | tf_op jit(solution)/shard_map/all_gather | solution.py:28
  242.8 81.3 %all-gather.21.cloned.1.call-start = ((), (), s32[]{:S(2)}) async-start(), calls=%async_computation.9 | async-start | bytes 1310720 | tf_op jit(solution)/shard_map/all_gather | solution.py:28
  267.4 29.9 %copy-start.4 = (f32[16,128,128]{2,1,0:T(8,128)S(1)}, f32[16,128,128]{2,1,0:T(8,128)}, u32[]{:S(2)}) copy-start(f32[16,128,128]{2,1,0:T(8,128)} %all-gather.13.cloned.1.call-done) | copy-start | bytes 3145732
  293.5 3.8 copy-start.43
  295.0 4.5 copy-start.21
  296.5 0.7 copy-start.29
  297.7 0.7 copy-start.31
  299.5 50.6 %all-gather.15.cloned.1.call-start = ((), (), s32[]{:S(2)}) async-start(), calls=%async_computation.6 | async-start | bytes 1310720 | tf_op jit(solution)/shard_map/all_gather | solution.py:28
  299.9 0.7 copy-start.23
  300.6 2.7 copy-start.48
  301.0 3.2 copy-start.14
  301.4 0.7 copy-start.16
  303.2 5.6 copy-start.46
  303.3 83.9 %all-gather.23.cloned.1.call-start = ((), (), s32[]{:S(2)}) async-start(), calls=%async_computation.10 | async-start | bytes 1310720 | tf_op jit(solution)/shard_map/all_gather | solution.py:28
  350.1 3.8 copy-start.3
  350.1 3.8 copy-start.42
  351.7 4.5 copy-start.25
  353.2 0.7 copy-start.33
  354.3 0.7 copy-start.35
  356.2 50.9 %all-gather.17.cloned.1.call-start = ((), (), s32[]{:S(2)}) async-start(), calls=%async_computation.7 | async-start | bytes 1310720 | tf_op jit(solution)/shard_map/all_gather | solution.py:28
  365.3 2.9 copy-start.12
  368.5 0.7 copy-start.18
  369.2 2.6 copy-start.53
  370.0 0.7 copy-start.9
  371.8 10.4 %copy-start.6 = (f32[8,64,4,128]{3,2,1,0:T(4,128)S(1)}, f32[8,64,4,128]{3,2,1,0:T(4,128)}, u32[]{:S(2)}) copy-start(f32[8,64,4,128]{3,2,1,0:T(4,128)} %reshape.171) | copy-start | bytes 3145732
  377.7 4.5 copy-start.13
  377.7 4.5 copy-start.39
  382.2 2.1 copy-start.15
  382.2 2.1 copy-start.17
  382.2 2.1 copy-start.20
  382.2 2.1 copy-start.24
  382.3 2.5 copy-start.26
  382.3 2.5 copy-start.28
  382.3 2.5 copy-start.34
  382.3 2.5 copy-start.36
  384.4 1.6 copy-start.10
  384.4 1.6 copy-start.11
  384.4 1.6 copy-start.19
  407.1 2.9 copy-start.7
  410.0 3.0 copy-start.38
  410.0 3.4 copy-start.22
  410.0 3.4 copy-start.27
  410.0 3.4 copy-start.30
  410.0 3.4 copy-start.32
  410.0 3.4 copy-start.44
  411.5 2.3 copy-start.8
  462.8 1.3 copy-start.47
  471.4 4.9 copy-start.49
  475.3 1.0 copy-start.40
  569.9 58.2 %all-to-all-start.3 = ((bf16[128,6,2048]{2,1,0:T(8,128)(2,1)}), bf16[128,6,2048]{2,1,0:T(8,128)(2,1)}, u32[]{:S(2)}, u32[]{:S(2)}) async-start(bf16[128,6,2048]{2,1,0:T(8,128)(2,1)} %get-tuple-element.230), calls=%async_computation.3 | async-start | bytes 8388608 | tf_op jit(solution)/shard_map/all_to_all | solution.py:51
  628.1 58.2 %all-to-all-start.2 = ((bf16[128,6,2048]{2,1,0:T(8,128)(2,1)}), bf16[128,6,2048]{2,1,0:T(8,128)(2,1)}, u32[]{:S(2)}, u32[]{:S(2)}) async-start(bf16[128,6,2048]{2,1,0:T(8,128)(2,1)} %reshape.174), calls=%async_computation.2 | async-start | bytes 8388608 | tf_op jit(solution)/shard_map/all_to_all | solution.py:254
  659.9 32.4 %copy-start.51 = (f32[256,4]{0,1:T(4,128)S(1)}, f32[256,4]{0,1:T(4,128)}, u32[]{:S(2)}) copy-start(f32[256,4]{0,1:T(4,128)} %param.37) | copy-start | bytes 12292
  659.9 32.6 %copy-start.41 = (bf16[256,2048]{1,0:T(8,128)(2,1)S(1)}, bf16[256,2048]{1,0:T(8,128)(2,1)}, u32[]{:S(2)}) copy-start(bf16[256,2048]{1,0:T(8,128)(2,1)} %copy-done.40) | copy-start | bytes 3145732
  686.4 58.5 %all-to-all-start.4 = ((bf16[128,6,2048]{2,1,0:T(8,128)(2,1)}), bf16[128,6,2048]{2,1,0:T(8,128)(2,1)}, u32[]{:S(2)}, u32[]{:S(2)}) async-start(bf16[128,6,2048]{2,1,0:T(8,128)(2,1)} %reshape.176), calls=%async_computation.4 | async-start | bytes 8388608 | tf_op jit(solution)/shard_map/all_to_all | solution.py:254
Sparse Core Ops, SparseCore 0:
  242.2 25.1 all-gather.12
  269.1 24.4 all-gather.18
  299.6 24.4 all-gather.20
  325.7 24.4 all-gather.14
  356.3 24.6 all-gather.22
  382.5 24.5 all-gather.16
where the time goes:
time: 816 us; the launch traced here: 805 us
  waiting for transfers between devices  213 us (26%)
  other arithmetic  199 us (24%)
  matrix products  161 us (20%)
  local copies, waits for them, and re-layouts  131 us (16%)
  blocking collectives  67.7 us (8%)
  starting transfers between devices  17.6 us (2%)
  between operations  14.8 us (2%)
    another operation x4, other arithmetic, block_terms(): jax.scipy.linalg.solve_triangular(lower, right, lower=True, unit_diagonal...  159 us
    all_gather x6, waiting for transfers between devices, entering(): pieces = jax.tree.map(lambda part: lax.all_gather(part, axis), running)  110 us
    all_to_all x2, waiting for transfers between devices, serve(): lax.all_to_all(expert_ffn(arrived), SP_TP, split_axis=0, concat_axis=0, t...  75.6 us
    all_to_all x1, blocking collectives, items_in_groups(): lax.all_to_all(group, axis, split_axis=split_dim, concat_axis=concat_dim,...  61 us
    all_to_all x1, waiting for transfers between devices, items_in_groups(): lax.all_to_all(group, axis, split_axis=split_dim, concat_axis=concat_dim,...  26.4 us
    dot_general x3, matrix products, feed_forward(): return jnp.dot(hidden, w_down, preferred_element_type=jnp.float32)  22.1 us
    reshape x2, local copies, waits for them, and re-layouts, shards(): back.reshape(experts * room, -1)[target].reshape(length, TOP_K, -1)  17.9 us
    gather x2, local copies, waits for them, and re-layouts, shards(): normed[source]  17.7 us
  transfers between devices with their start and end apart: 9, of which 8 were waited for; matrix products, arithmetic and copies ran while one was open for 12% of the time, Pallas kernels for 0%

commit v1 on v0

v1 whole, which is shorter than its diff:
```python
import jax
import jax.numpy as jnp
from jax import lax
from jax.experimental import pallas as pl
from jax.experimental.pallas import tpu as pltpu
from jax.sharding import Mesh
from jax.sharding import PartitionSpec as P

TOP_K = 4
HD = 128
BLOCK = 128
KEEP = 8
SP = ("sp_0", "sp_1", "sp_2")
SP_TP = ("sp_0", "sp_1", "sp_2", "tp")
EPS = 1e-06
F32 = jnp.float32
BF16 = jnp.bfloat16


def dot_nn(a, b):
    return lax.dot_general(a, b, (((1,), (0,)), ((), ())), preferred_element_type=F32)


def dot_nt(a, b):
    return lax.dot_general(a, b, (((1,), (1,)), ((), ())), preferred_element_type=F32)


def dot_tn(a, b):
    return lax.dot_general(a, b, (((0,), (0,)), ((), ())), preferred_element_type=F32)


def parts(x):
    high = x.astype(BF16)
    return high, (x - high.astype(F32)).astype(BF16)


def rows_of(*arrays):
    return jnp.concatenate(arrays, axis=0)


def cols_of(*arrays):
    return jnp.concatenate(arrays, axis=1)


def fine(a, b):
    ah, al = a
    bh, bl = b
    return dot_nn(cols_of(ah, al), rows_of(bh, bh)) + dot_nn(ah, bl)


def fine_square(a, b):
    ah, al = a
    bh, bl = b
    both = dot_nn(cols_of(ah, al), rows_of(cols_of(bh, bl), cols_of(bh, jnp.zeros_like(bl))))
    return both[:, :HD] + both[:, HD:]


def sub(pair, rows):
    return pair[0][rows], pair[1][rows]


def terms_kernel(q_ref, k_ref, v_ref, ldb_ref, mb_ref, qe_ref, o0_ref):
    length = q_ref.shape[0]
    number = length // BLOCK
    rows = ldb_ref[0]
    lane = lax.broadcasted_iota(jnp.int32, rows.shape, 1)
    total = rows
    shift = 1
    while shift < length:
        total = total + jnp.where(lane >= shift, pltpu.roll(total, shift, 1), 0.0)
        shift *= 2
    g_row = total[0:1, :]
    g_col = jnp.broadcast_to(g_row, (HD, length)).T
    b_col = jnp.broadcast_to(rows[1:2, :], (HD, length)).T

    def unit(ref):
        x = ref[...].astype(F32)
        active = x * jax.nn.sigmoid(x)
        return active * lax.rsqrt(jnp.sum(active * active, axis=-1, keepdims=True) + EPS)

    queries = unit(q_ref)
    keys = unit(k_ref)
    raw = v_ref[...].astype(F32)
    values = raw * jax.nn.sigmoid(raw)
    grown = jnp.exp(g_col)
    k_beta = keys * b_col
    right = cols_of(k_beta * grown, values * b_col)
    g_last = g_col[length - 1 : length, :]
    k_late = parts(keys * jnp.exp(g_last - g_col))
    qs, ks, kbs = parts(queries), parts(keys), parts(k_beta)
    ii = lax.broadcasted_iota(jnp.int32, (BLOCK, BLOCK), 0)
    jj = lax.broadcasted_iota(jnp.int32, (BLOCK, BLOCK), 1)
    lower, mixing, solved = [], [], []
    for r in range(number):
        here = slice(r * BLOCK, (r + 1) * BLOCK)
        upto = slice(0, (r + 1) * BLOCK)
        left = rows_of(cols_of(kbs[0][here], kbs[1][here]), cols_of(qs[0][here], qs[1][here]))
        high = ks[0][upto]
        both = dot_nt(left, cols_of(high, high)) + dot_nt(rows_of(kbs[0][here], qs[0][here]), ks[1][upto])
        a_row, p_row = [], []
        for c in range(r + 1):
            there = slice(c * BLOCK, (c + 1) * BLOCK)
            gap = g_col[here] - g_row[:, there]
            if c == r:
                gap = jnp.where(ii >= jj, gap, -1e30)
            fade = jnp.exp(gap)
            a_one = both[:BLOCK, there] * fade
            if c == r:
                a_one = jnp.where(ii > jj, a_one, 0.0)
            a_row.append(a_one)
            p_row.append(both[BLOCK:, there] * fade)
        lower.append(a_row)
        mixing.append(p_row)
    eye = (ii == jj).astype(F32)
    inverse = [eye - jnp.where((ii // 2 == jj // 2) & (ii > jj), lower[r][r], 0.0) for r in range(number)]
    size = 2
    while size < BLOCK:
        chosen = (ii // (2 * size) == jj // (2 * size)) & (ii // size > jj // size)
        halves = [parts(t) for t in inverse]
        steps = [
            fine_square(halves[r], parts(jnp.where(chosen, lower[r][r], 0.0))) for r in range(number)
        ]
        inverse = [inverse[r] - fine_square(parts(steps[r]), halves[r]) for r in range(number)]
        size *= 2
    highs, lows = [], []
    for r in range(number):
        here = slice(r * BLOCK, (r + 1) * BLOCK)
        rest = right[here]
        if r > 0:
            known = (rows_of(*highs), rows_of(*lows))
            rest = rest - fine(parts(cols_of(*lower[r][:r])), known)
        one = parts(fine(parts(inverse[r]), parts(rest)))
        highs.append(one[0])
        lows.append(one[1])
        known = (rows_of(*highs), rows_of(*lows))
        mixed = fine(parts(cols_of(*mixing[r])), known)
        qe_ref[here, :] = queries[here] * grown[here] - mixed[:, :HD]
        o0_ref[here, :] = mixed[:, HD:]
    known = (rows_of(*highs), rows_of(*lows))
    moved = dot_tn(rows_of(*k_late), rows_of(known[0], known[0])) + dot_tn(k_late[0], known[1])
    mb_ref[0, :, :HD] = eye * jnp.exp(g_last) - moved[:, :HD]
    mb_ref[0, :, HD:] = moved[:, HD:]


def block_terms(queries, keys, values, log_decay, beta):
    length, wide = queries.shape
    heads = wide // HD
    pad = jnp.zeros((heads, 6, length), F32)
    table = jnp.concatenate([log_decay.T[:, None, :], beta.T[:, None, :], pad], axis=1)
    column = pl.BlockSpec((length, HD), lambda h: (0, h))
    return pl.pallas_call(
        terms_kernel,
        grid=(heads,),
        in_specs=[column, column, column, pl.BlockSpec((1, 8, length), lambda h: (h, 0, 0))],
        out_specs=[pl.BlockSpec((1, HD, 2 * HD), lambda h: (h, 0, 0)), column, column],
        out_shape=[
            jax.ShapeDtypeStruct((heads, HD, 2 * HD), F32),
            jax.ShapeDtypeStruct((length, wide), F32),
            jax.ShapeDtypeStruct((length, wide), F32),
        ],
        name="terms",
    )(queries, keys, values, table)


def shift_in(later):
    wide = lax.broadcasted_iota(jnp.int32, later.shape, 1)
    return jnp.where(wide >= HD, later, 0.0)


def then(later, earlier):
    return fine(parts(later[:, :HD]), parts(earlier)) + shift_in(later)


def identity_map():
    ii = lax.broadcasted_iota(jnp.int32, (HD, 2 * HD), 0)
    jj = lax.broadcasted_iota(jnp.int32, (HD, 2 * HD), 1)
    return (ii == jj).astype(F32)


def all_before_kernel(x_ref, before_ref, total_ref):
    running = identity_map()
    for k in range(x_ref.shape[0]):
        before_ref[k] = running
        running = x_ref[k] if k == 0 else then(x_ref[k], running)
    total_ref[...] = running


def all_before(maps):
    return pl.pallas_call(
        all_before_kernel,
        out_shape=[
            jax.ShapeDtypeStruct(maps.shape, F32),
            jax.ShapeDtypeStruct(maps.shape[1:], F32),
        ],
        name="all_before",
    )(maps)


def mine_before_kernel(mine_ref, x_ref, before_ref, total_ref):
    mine = mine_ref[0]
    running = identity_map()
    before_ref[...] = running
    for k in range(x_ref.shape[0]):
        running = x_ref[k] if k == 0 else then(x_ref[k], running)

        @pl.when(mine == k + 1)
        def _(running=running):
            before_ref[...] = running

    total_ref[...] = running


def mine_before(maps, mine):
    one = jax.ShapeDtypeStruct(maps.shape[1:], F32)
    return pl.pallas_call(
        mine_before_kernel,
        in_specs=[
            pl.BlockSpec(memory_space=pltpu.SMEM),
            pl.BlockSpec(memory_space=pltpu.VMEM),
        ],
        out_shape=[one, one],
        name="mine_before",
    )(mine, maps)


def states_kernel(mine_ref, outer_ref, middle_ref, inner_ref, out_ref, state_ref):
    mine = mine_ref[0]
    state_ref[...] = jnp.zeros_like(state_ref)
    for k in range(outer_ref.shape[0] - 1):

        @pl.when(mine > k)
        def _(k=k):
            state_ref[...] = (
                fine(parts(outer_ref[k, :, :HD]), parts(state_ref[...])) + outer_ref[k, :, HD:]
            )

    state = fine(parts(middle_ref[:, :HD]), parts(state_ref[...])) + middle_ref[:, HD:]
    pair = parts(state)
    out_ref[0] = state
    for k in range(1, inner_ref.shape[0]):
        out_ref[k] = fine(parts(inner_ref[k, :, :HD]), pair) + inner_ref[k, :, HD:]


def states(outer, mine, middle, inner):
    return pl.pallas_call(
        states_kernel,
        in_specs=[pl.BlockSpec(memory_space=pltpu.SMEM)]
        + [pl.BlockSpec(memory_space=pltpu.VMEM)] * 3,
        out_shape=jax.ShapeDtypeStruct((inner.shape[0], HD, HD), F32),
        scratch_shapes=[pltpu.VMEM((HD, HD), F32)],
        name="states",
    )(mine, outer, middle, inner)


def entering(maps):
    by_position = lax.all_to_all(maps, "sp_2", split_axis=0, concat_axis=0, tiled=True)
    inner, line = all_before(by_position)
    lines = lax.all_gather(line, "sp_1")
    middle, plane = mine_before(lines, lax.axis_index("sp_1").reshape(1).astype(jnp.int32))
    planes = lax.all_gather(plane, "sp_0")
    found = states(planes, lax.axis_index("sp_0").reshape(1).astype(jnp.int32), middle, inner)
    return lax.all_to_all(found, "sp_2", split_axis=0, concat_axis=0, tiled=True)


def finish_kernel(qe_ref, o0_ref, s_ref, gate_ref, gain_ref, out_ref):
    mix = o0_ref[...] + fine(parts(qe_ref[...]), parts(s_ref[0]))
    scaled = mix * lax.rsqrt(jnp.mean(mix * mix, axis=-1, keepdims=True) + EPS)
    gate = gate_ref[...].astype(F32)
    out_ref[...] = (scaled * gain_ref[...] * (gate * jax.nn.sigmoid(gate))).astype(BF16)


def finish(qe, o0, state, gate, gain):
    length, wide = qe.shape
    column = pl.BlockSpec((length, HD), lambda h: (0, h))
    return pl.pallas_call(
        finish_kernel,
        grid=(wide // HD,),
        in_specs=[
            column,
            column,
            pl.BlockSpec((1, HD, HD), lambda h: (h, 0, 0)),
            column,
            pl.BlockSpec((1, HD), lambda h: (0, 0)),
        ],
        out_specs=column,
        out_shape=jax.ShapeDtypeStruct((length, wide), BF16),
        name="finish",
    )(qe, o0, state, gate, gain.reshape(1, HD))


def normalize(wide, gain):
    return (wide * lax.rsqrt(jnp.mean(wide * wide, axis=-1, keepdims=True) + EPS) * gain).astype(
        BF16
    )


def feed_forward(rows, w_gate, w_up, w_down):
    hidden = jax.nn.silu(jnp.dot(rows, w_gate, preferred_element_type=F32))
    hidden = (hidden * jnp.dot(rows, w_up, preferred_element_type=F32)).astype(BF16)
    return jnp.dot(hidden, w_down, preferred_element_type=F32)


def exchange(rows):
    return lax.all_to_all(rows, SP_TP, split_axis=0, concat_axis=0, tiled=True)


def routes(index, weight, experts, room):
    length = index.shape[0]
    ids = jnp.arange(experts, dtype=jnp.int32)[:, None]
    named = jnp.zeros((experts, length), F32)
    weights = jnp.zeros((experts, length), F32)
    for j in range(index.shape[1]):
        here = index[:, j][None, :] == ids
        named = named + here.astype(F32)
        weights = weights + jnp.where(here, weight[:, j][None, :], 0.0)
    place = jnp.arange(length, dtype=jnp.int32)
    earlier = (place[:, None] < place[None, :]).astype(BF16)
    slot = jnp.dot(named.astype(BF16), earlier, preferred_element_type=F32)
    slot = jnp.where(named > 0, slot, -1.0)[:, None, :]
    step = jnp.arange(KEEP, dtype=jnp.int32)[None, :, None]
    extra = room - KEEP
    first = slot == step.astype(F32)
    rest = slot == (KEEP + step % extra).astype(F32)
    lead = rest & (step < extra)
    tail = rest & (step >= extra)
    weights = weights[:, None, :]

    def flat(mask):
        return mask.reshape(experts * KEEP, length)

    out = [flat(m.astype(BF16)) for m in (first, lead, tail)]
    back = [flat(jnp.where(m, weights, 0.0).astype(BF16)) for m in (first, lead, tail)]
    return out, back


def shards(
    projected_queries,
    projected_keys,
    projected_values,
    output_gate_values,
    write_strength_logits,
    decay_input_logits,
    head_rate_logarithm,
    extra_log_decay,
    per_head_norm_gain,
    output_matrix,
    residual,
    mixture_norm_gain,
    selected_expert_index,
    routing_weight,
    routed_gate_weight,
    routed_up_weight,
    routed_down_weight,
    common_gate_weight,
    common_up_weight,
    common_down_weight,
):
    beta = jax.nn.sigmoid(write_strength_logits.astype(F32))
    log_decay = extra_log_decay - jnp.exp(head_rate_logarithm)[None, :] * jax.nn.softplus(
        decay_input_logits.astype(F32) - 6.0
    )
    maps, qe, o0 = block_terms(projected_queries, projected_keys, projected_values, log_decay, beta)
    state = entering(maps)
    heads_out = finish(qe, o0, state, output_gate_values, per_head_norm_gain)
    length = residual.shape[0]
    wide = heads_out.shape[1]
    pieces = lax.all_to_all(
        heads_out.reshape(2, length, wide), "tp", split_axis=0, concat_axis=0, tiled=True
    )
    projected = jnp.dot(pieces[0], output_matrix[:wide], preferred_element_type=F32) + jnp.dot(
        pieces[1], output_matrix[wide:], preferred_element_type=F32
    )
    attended = (residual.astype(F32) + projected).astype(BF16)
    normed = normalize(attended.astype(F32), mixture_norm_gain)

    experts = lax.axis_size(SP) * lax.axis_size("tp")
    room = max(2, length * TOP_K * 3 // (2 * experts))
    extra = room - KEEP
    dim = normed.shape[1]
    half = dim // 2
    (first, lead, tail), (w_first, w_lead, w_tail) = routes(
        selected_expert_index, routing_weight, experts, room
    )
    main_out = jnp.dot(first, normed, preferred_element_type=F32).astype(BF16)
    rest_out = (
        jnp.dot(lead, normed[:, :half], preferred_element_type=F32)
        + jnp.dot(tail, normed[:, half:], preferred_element_type=F32)
    ).astype(BF16)
    main_in = exchange(main_out.reshape(experts, KEEP, dim))
    rest_in = exchange(rest_out.reshape(experts, KEEP, half))
    shared = feed_forward(normed, common_gate_weight, common_up_weight, common_down_weight)

    weights = (routed_gate_weight[0], routed_up_weight[0], routed_down_weight[0])
    main_rows = feed_forward(main_in.reshape(experts * KEEP, dim), *weights).astype(BF16)
    main_back = exchange(main_rows.reshape(experts, KEEP, dim)).reshape(experts * KEEP, dim)
    unfolded = rest_in.reshape(experts, 2, extra, half).transpose(0, 2, 1, 3)
    rest_rows = feed_forward(unfolded.reshape(experts * extra, dim), *weights).astype(BF16)
    folded = rest_rows.reshape(experts, extra, 2, half).transpose(0, 2, 1, 3)
    rest_back = exchange(folded.reshape(experts, KEEP, half)).reshape(experts * KEEP, half)

    def combine(table, rows):
        return lax.dot_general(table, rows, (((0,), (0,)), ((), ())), preferred_element_type=F32)

    routed = combine(w_first, main_back) + jnp.concatenate(
        [combine(w_lead, rest_back), combine(w_tail, rest_back)], axis=1
    )
    return (attended.astype(F32) + shared + routed).astype(BF16)


def solution(mesh):
    finer = Mesh(mesh.devices.reshape(4, 4, 4, mesh.shape["tp"]), ("sp_0", "sp_1", "sp_2", "tp"))
    in_specs = (
        P(SP, "tp"),
        P(SP, "tp"),
        P(SP, "tp"),
        P(SP, "tp"),
        P(SP, "tp"),
        P(SP, "tp"),
        P("tp"),
        P(SP, "tp"),
        P(),
        P(),
        P(SP_TP, None),
        P(),
        P(SP_TP, None),
        P(SP_TP, None),
        P(SP_TP, None, None),
        P(SP_TP, None, None),
        P(SP_TP, None, None),
        P(),
        P(),
        P(),
    )
    out_specs = P(SP_TP, None)
    return jax.shard_map(
        shards, mesh=finer, in_specs=in_specs, out_specs=out_specs, check_vma=False
    )
```

time: 816 us -> 305 us (0.37); the launches traced: 805 us -> 304 us
  other arithmetic: 199 us -> 2.74 us
  local copies, waits for them, and re-layouts: 131 us -> 22.6 us
  matrix products: 161 us -> 55.1 us
  waiting for transfers between devices: 213 us -> 121 us
  Pallas kernels: 0 us -> 31.5 us
  blocking collectives: 67.7 us -> 39.9 us
  between operations: 14.8 us -> 0.24 us
  starting transfers between devices: 17.6 us -> 30.5 us
    another operation x5 -> x0, other arithmetic: 160 us -> none  [the longest x4 159 us: block_terms(): jax.scipy.linalg.solve_triangular(lower, right, lower=True, unit_diagonal...]
    all_gather x6 -> x0, waiting for transfers between devices: 110 us -> none  [entering(): pieces = jax.tree.map(lambda part: lax.all_gather(part, axis), running)]
    dot_general x100 -> x15, matrix products: 159 us -> 55.1 us  [the longest x3 22 us: feed_forward(): return jnp.dot(hidden, w_down, preferred_element_type=F32)]
    all_to_all x2 -> x1, blocking collectives: 67.7 us -> 12.6 us  [shards(): lax.all_to_all(heads_out.reshape(2, length, wide), 'tp', split_axis=0, co...]
    reshape x8 -> x2, local copies, waits for them, and re-layouts: 48.3 us -> 8.5 us  [the longest x1 4.51 us: shards(): folded = rest_rows.reshape(experts, extra, 2, half).transpose(0, 2, 1, 3)]
    pallas_call x0 -> x5, Pallas kernels: none -> 31.5 us  [the longest x1 20 us: block_terms(): pl.pallas_call(terms_kernel, grid=(heads,), in_specs=[column, column, col...]
    gather x3 -> x0, local copies, waits for them, and re-layouts: 30.1 us -> none  [the longest x2 17.7 us: shards(): normed[source]]
    all_gather x0 -> x2, blocking collectives: none -> 27.3 us  [the longest x1 13.8 us: entering(): lines = lax.all_gather(line, 'sp_1')]
  transfers between devices with their start and end apart: 9 -> 6, of which waited for: 8 -> 6; matrix products, arithmetic and copies ran while one was open for 12% -> 19% of each run, Pallas kernels for 0% -> 0%
where the time goes in v1:
time: 305 us; the launch traced here: 304 us
  waiting for transfers between devices  121 us (40%)
  matrix products  55.1 us (18%)
  blocking collectives  39.9 us (13%)
  Pallas kernels  31.5 us (10%)
  starting transfers between devices  30.5 us (10%)
  local copies, waits for them, and re-layouts  22.6 us (7%)
    all_to_all x4, waiting for transfers between devices, exchange(): return lax.all_to_all(rows, SP_TP, split_axis=0, concat_axis=0, tiled=True)  108 us
    all_to_all x4, starting transfers between devices, exchange(): return lax.all_to_all(rows, SP_TP, split_axis=0, concat_axis=0, tiled=True)  22.2 us
    dot_general x3, matrix products, feed_forward(): return jnp.dot(hidden, w_down, preferred_element_type=F32)  22 us
    pallas_call x1, Pallas kernels, block_terms(): pl.pallas_call(terms_kernel, grid=(heads,), in_specs=[column, column, col...  20 us
    all_gather x1, blocking collectives, entering(): lines = lax.all_gather(line, 'sp_1')  13.8 us
    all_gather x1, blocking collectives, entering(): planes = lax.all_gather(plane, 'sp_0')  13.5 us
    all_to_all x1, blocking collectives, shards(): lax.all_to_all(heads_out.reshape(2, length, wide), 'tp', split_axis=0, co...  12.6 us
    dot_general x3, matrix products, feed_forward(): hidden = jax.nn.silu(jnp.dot(rows, w_gate, preferred_element_type=F32))  11.9 us
  transfers between devices with their start and end apart: 6, of which 6 were waited for; matrix products, arithmetic and copies ran while one was open for 19% of the time, Pallas kernels for 0%

profile of v1, /device:TPU:1, one launch (start us, length us, event | category | flops | bytes accessed | tf_op | source)
XLA Modules:
  0.0 304.1 jit_solution(12983077006165008361)
XLA Ops:
  0.0 0.0 copy-start
  0.0 0.9 divide_bitcast_fusion
  0.9 0.7 exp.22
  1.5 0.8 fusion.87
  2.3 0.1 pad.4.clone
  2.4 0.7 maximum_maximum_fusion.ldb_ref
  3.1 20.0 %terms.1 = (f32[4,128,256]{2,1,0:T(8,128)}, f32[512,512]{1,0:T(8,128)}, f32[512,512]{1,0:T(8,128)}) custom-call(bf16[512,512]{1,0:T(8,128)(2,1)} %q_ref.1, bf16[512,512]{1,0:T(8,128)(2,1)} %k_ref.1, bf16[512,512]{1,0:T(8,128)(2,1)} %v_ref.1, f32[4,8,512]{2,1,0:T(8,128)} %maximum_maximum_fusion.ldb_ref), custom_call_target="tpu_custom_call" | custom-call | tf_op jit(solution)/shard_map/terms/pallas_call | solution.py:151
  23.1 4.8 %all-to-all-start = ((f32[4,128,256]{2,1,0:T(8,128)}), f32[4,128,256]{2,1,0:T(8,128)S(1)}, u32[]{:S(2)}, u32[]{:S(2)}) async-start(f32[4,128,256]{2,1,0:T(8,128)} %get-tuple-element.14), calls=%async_computation | async-start | bytes 1048576 | tf_op jit(solution)/shard_map/all_to_all | solution.py:256
  28.0 0.1 eq.150
  28.1 0.1 and.55
  28.2 0.1 and.59
  28.4 0.0 copy-done.8
  28.4 7.9 %all-to-all-done.x_ref = f32[4,128,256]{2,1,0:T(8,128)S(1)} async-done(((f32[4,128,256]{2,1,0:T(8,128)}), f32[4,128,256]{2,1,0:T(8,128)S(1)}, u32[]{:S(2)}, u32[]{:S(2)}) %all-to-all-start) | async-done | bytes 524320 | tf_op jit(solution)/shard_map/all_to_all | solution.py:256
  36.3 0.8 copy-done.4
  37.1 2.4 all_before.1
  39.5 13.8 %all-gather = f32[512,256]{1,0:T(8,128)} all-gather(f32[128,256]{1,0:T(8,128)} %get-tuple-element.15), channel_id=2, replica_groups=mesh['sp_0'=4,'sp_1'=4,'sp_2'=4,'tp'=2] {'sp_1'}, dimensions={0}, use_global_device_ids=true | all-gather | bytes 655360 | tf_op jit(solution)/shard_map/all_gather | solution.py:258
  53.3 2.4 mine_before.1
  55.7 13.5 %all-gather.1 = f32[512,256]{1,0:T(8,128)} all-gather(f32[128,256]{1,0:T(8,128)} %get-tuple-element.16), channel_id=3, replica_groups=mesh['sp_0'=4,'sp_1'=4,'sp_2'=4,'tp'=2] {'sp_0'}, dimensions={0}, use_global_device_ids=true | all-gather | bytes 655360 | tf_op jit(solution)/shard_map/all_gather | solution.py:260
  69.1 2.4 states.1
  71.6 3.4 %all-to-all-start.1 = ((f32[4,128,128]{2,1,0:T(8,128)}), f32[4,128,128]{2,1,0:T(8,128)S(1)}, u32[]{:S(2)}, u32[]{:S(2)}) async-start(f32[4,128,128]{2,1,0:T(8,128)} %states.1), calls=%async_computation.1 | async-start | bytes 524288 | tf_op jit(solution)/shard_map/all_to_all | solution.py:262
  75.0 0.2 convolution_select_fusion
  75.2 5.3 %all-to-all-done.1.s_ref = f32[4,128,128]{2,1,0:T(8,128)S(1)} async-done(((f32[4,128,128]{2,1,0:T(8,128)}), f32[4,128,128]{2,1,0:T(8,128)S(1)}, u32[]{:S(2)}, u32[]{:S(2)}) %all-to-all-start.1) | async-done | bytes 262176 | tf_op jit(solution)/shard_map/all_to_all | solution.py:262
  80.5 0.7 copy-done.5
  81.2 4.3 %finish.1 = bf16[512,512]{1,0:T(8,128)(2,1)} custom-call(f32[512,512]{1,0:T(8,128)} %get-tuple-element.12.qe_ref, f32[512,512]{1,0:T(8,128)} %get-tuple-element.13.o0_ref, f32[4,128,128]{2,1,0:T(8,128)} %copy-done.5, bf16[512,512]{1,0:T(8,128)(2,1)} %gate_ref.1, f32[1,128]{1,0:T(1,128)} %bitcast.119), custom_call_target="tpu_custom_call" | custom-call | tf_op jit(solution)/shard_map/finish/pallas_call | solution.py:275
  85.5 12.6 %all_to_all.35 = bf16[2,256,512]{2,1,0:T(8,128)(2,1)S(1)} all-to-all(bf16[2,256,512]{2,1,0:T(8,128)(2,1)} %bitcast.106), channel_id=1, replica_groups=mesh['sp_0'=4,'sp_1'=4,'sp_2'=4,'tp'=2] {'tp'}, dimensions={0} | all-to-all | bytes 1048576 | tf_op jit(solution)/shard_map/all_to_all | solution.py:367
  98.1 2.4 fusion.21
  100.6 0.0 copy-done.6
  100.6 0.4 copy-done.2
  101.0 0.9 fusion.9
  101.9 0.0 copy-done.7
  101.9 0.3 fusion.11
  102.2 0.8 fusion.42
  103.0 2.3 fusion.23
  105.3 5.7 %all-to-all-start.5 = ((bf16[128,8,1024]{2,1,0:T(8,128)(2,1)}), bf16[128,8,1024]{2,1,0:T(8,128)(2,1)}, u32[]{:S(2)}, u32[]{:S(2)}) async-start(bf16[128,8,1024]{2,1,0:T(8,128)(2,1)} %fusion.23), calls=%async_computation.5 | async-start | bytes 4194304 | tf_op jit(solution)/shard_map/all_to_all | solution.py:304
  111.0 0.1 eq.144
  111.1 3.4 %convert_bitcast_fusion.1 = bf16[128,8,2048]{2,1,0:T(8,128)(2,1)} fusion(f32[1024]{0:T(1024)S(1)} %eq.144, f32[128,256]{1,0:T(8,128)S(1)} %convolution_select_fusion, bf16[256,2048]{1,0:T(8,128)(2,1)S(1)} %get-tuple-element.28, f32[2048]{0:T(1024)S(1)} %copy-done.7, f32[256]{0:T(256)S(1)} %add_rsqrt_fusion), kind=kOutput, calls=%fused_computation.6 | convolution fusion | flops 1078198272 | bytes 5387264 | tf_op jit(solution)/shard_map/dot_general | solution.py:384
  114.5 26.6 %all-to-all-done.5 = bf16[128,8,1024]{2,1,0:T(8,128)(2,1)} async-done(((bf16[128,8,1024]{2,1,0:T(8,128)(2,1)}), bf16[128,8,1024]{2,1,0:T(8,128)(2,1)}, u32[]{:S(2)}, u32[]{:S(2)}) %all-to-all-start.5) | async-done | bytes 2097184 | tf_op jit(solution)/shard_map/all_to_all | solution.py:304
  141.1 5.5 %all-to-all-start.3 = ((bf16[128,8,2048]{2,1,0:T(8,128)(2,1)}), bf16[128,8,2048]{2,1,0:T(8,128)(2,1)}, u32[]{:S(2)}, u32[]{:S(2)}) async-start(bf16[128,8,2048]{2,1,0:T(8,128)(2,1)} %convert_bitcast_fusion.1), calls=%async_computation.3 | async-start | bytes 8388608 | tf_op jit(solution)/shard_map/all_to_all | solution.py:304
  146.6 2.7 copy.33
  149.4 2.2 copy.34
  151.5 0.0 copy-start.10
  151.6 0.6 copy.36
  152.2 0.0 copy-start.3
  152.2 1.3 copy-done.3
  153.5 0.0 copy-done.10
  153.5 2.2 fusion.17
  155.7 6.3 %convolution_convert_fusion = bf16[512,2048]{1,0:T(8,128)(2,1)} fusion(bf16[1,512,2048]{2,1,0:T(8,128)(2,1)S(1)} %copy-done, bf16[512,2048]{1,0:T(8,128)(2,1)} %bitcast.105, bf16[1,2048,512]{2,1,0:T(8,128)(2,1)} %param.35, f32[512,512]{1,0:T(8,128)} %fusion.17), kind=kOutput, calls=%fused_computation.10 | convolution fusion | flops 2150105088 | bytes 9437184 | tf_op jit(solution)/shard_map/dot_general | solution.py:300
  162.0 4.5 %reshape.250 = bf16[128,4,2,1024]{3,2,1,0:T(2,128)(2,1)} reshape(bf16[512,2048]{1,0:T(8,128)(2,1)} %convolution_convert_fusion) | data formatting | bytes 4194304 | tf_op jit(solution)/shard_map/reshape | solution.py:398
  166.6 4.2 %copy.35 = bf16[128,2,4,1024]{3,2,1,0:T(4,128)(2,1)} copy(bf16[128,2,4,1024]{3,1,2,0:T(2,128)(2,1)} %bitcast.101) | data formatting | bytes 4194304 | tf_op jit(solution)/shard_map/transpose | solution.py:398
  170.7 4.0 %reshape.251 = bf16[128,8,1024]{2,1,0:T(8,128)(2,1)} reshape(bf16[128,2,4,1024]{3,2,1,0:T(4,128)(2,1)} %copy.35) | data formatting | bytes 4194304 | tf_op jit(solution)/shard_map/reshape | solution.py:399
  174.7 24.6 %all-to-all-done.3 = bf16[128,8,2048]{2,1,0:T(8,128)(2,1)} async-done(((bf16[128,8,2048]{2,1,0:T(8,128)(2,1)}), bf16[128,8,2048]{2,1,0:T(8,128)(2,1)}, u32[]{:S(2)}, u32[]{:S(2)}) %all-to-all-start.3) | async-done | bytes 4194336 | tf_op jit(solution)/shard_map/all_to_all | solution.py:304
  199.3 5.5 %all-to-all-start.6 = ((bf16[128,8,1024]{2,1,0:T(8,128)(2,1)}), bf16[128,8,1024]{2,1,0:T(8,128)(2,1)}, u32[]{:S(2)}, u32[]{:S(2)}) async-start(bf16[128,8,1024]{2,1,0:T(8,128)(2,1)} %reshape.251), calls=%async_computation.6 | async-start | bytes 4194304 | tf_op jit(solution)/shard_map/all_to_all | solution.py:304
  204.8 6.5 %fusion.2 = f32[1024,512]{1,0:T(8,128)} fusion(bf16[128,8,2048]{2,1,0:T(8,128)(2,1)} %all-to-all-done.3, bf16[1,2048,512]{2,1,0:T(8,128)(2,1)} %param.34), kind=kOutput, calls=%fused_computation.2 | convolution fusion | flops 2147483648 | bytes 8388608 | tf_op jit(solution)/shard_map/dot_general | solution.py:298
  211.3 10.1 %convert_bitcast_fusion = bf16[128,8,2048]{2,1,0:T(8,128)(2,1)} fusion(bf16[1,512,2048]{2,1,0:T(8,128)(2,1)S(1)} %copy-done, f32[1024,512]{1,0:T(8,128)} %fusion.2, bf16[1,2048,512]{2,1,0:T(8,128)(2,1)} %param.35, bf16[128,8,2048]{2,1,0:T(8,128)(2,1)} %all-to-all-done.3), kind=kOutput, calls=%fused_computation.5 | convolution fusion | flops 4300210176 | bytes 14680064 | tf_op jit(solution)/shard_map/dot_general | solution.py:300
  221.4 13.7 %all-to-all-done.6 = bf16[128,8,1024]{2,1,0:T(8,128)(2,1)} async-done(((bf16[128,8,1024]{2,1,0:T(8,128)(2,1)}), bf16[128,8,1024]{2,1,0:T(8,128)(2,1)}, u32[]{:S(2)}, u32[]{:S(2)}) %all-to-all-start.6) | async-done | bytes 2097184 | tf_op jit(solution)/shard_map/all_to_all | solution.py:304
  235.0 5.5 %all-to-all-start.4 = ((bf16[128,8,2048]{2,1,0:T(8,128)(2,1)}), bf16[128,8,2048]{2,1,0:T(8,128)(2,1)}, u32[]{:S(2)}, u32[]{:S(2)}) async-start(bf16[128,8,2048]{2,1,0:T(8,128)(2,1)} %convert_bitcast_fusion), calls=%async_computation.4 | async-start | bytes 8388608 | tf_op jit(solution)/shard_map/all_to_all | solution.py:304
  240.6 0.0 copy-done.9
  240.6 0.1 select_add_fusion
  240.7 3.2 %fusion.101 = f32[256,512]{1,0:T(8,128)} fusion(bf16[2048,512]{1,0:T(8,128)(2,1)} %param.37, bf16[256,2048]{1,0:T(8,128)(2,1)S(1)} %get-tuple-element.28, f32[2048]{0:T(1024)S(1)} %copy-done.7, f32[256]{0:T(256)S(1)} %add_rsqrt_fusion), kind=kOutput, calls=%fused_computation.119 | convolution fusion | flops 538968064 | bytes 3679232 | tf_op jit(solution)/shard_map/dot_general | solution.py:298
  243.8 2.5 convolution_bitcast_fusion.1
  246.3 3.5 %convolution_bitcast_fusion.2 = f32[256,1024]{1,0:T(8,128)} fusion(bf16[128,8,1024]{2,1,0:T(8,128)(2,1)} %all-to-all-done.6, bf16[128,256]{1,0:T(8,128)(2,1)S(1)} %select_add_fusion, f32[128,256]{1,0:T(8,128)S(1)} %convolution_select_fusion, f32[8]{0:T(128)S(1)} %fusion.89, pred[8]{0:T(512)(128)(4,1)S(1)} %iota_compare_fusion.7), kind=kOutput, calls=%fused_computation.37 | convolution fusion | flops 537657344 | bytes 3342376 | tf_op jit(solution)/shard_map/dot_general | solution.py:402
  249.8 43.4 %all-to-all-done.4 = bf16[128,8,2048]{2,1,0:T(8,128)(2,1)} async-done(((bf16[128,8,2048]{2,1,0:T(8,128)(2,1)}), bf16[128,8,2048]{2,1,0:T(8,128)(2,1)}, u32[]{:S(2)}, u32[]{:S(2)}) %all-to-all-start.4) | async-done | bytes 4194336 | tf_op jit(solution)/shard_map/all_to_all | solution.py:304
  293.3 5.2 %fusion.6 = f32[256,2048]{1,0:T(8,128)} fusion(bf16[128,8,2048]{2,1,0:T(8,128)(2,1)} %all-to-all-done.4, f32[256,1024]{1,0:T(8,128)S(1)} %convolution_bitcast_fusion.1, f32[256,1024]{1,0:T(8,128)} %convolution_bitcast_fusion.2, bf16[128,256]{1,0:T(8,128)(2,1)S(1)} %select_add_fusion, f32[128,256]{1,0:T(8,128)S(1)} %convolution_select_fusion, ...), kind=kOutput, calls=%fused_computation.15 | convolution fusion | flops 1075314688 | bytes 8585248 | tf_op jit(solution)/shard_map/dot_general | solution.py:402
  298.5 5.6 %fusion.8 = bf16[256,2048]{1,0:T(8,128)(2,1)} fusion(f32[256,2048]{1,0:T(8,128)} %fusion.6, bf16[512,2048]{1,0:T(8,128)(2,1)} %param.39, bf16[256,2048]{1,0:T(8,128)(2,1)S(1)} %get-tuple-element.28, bf16[2048,512]{1,0:T(8,128)(2,1)} %param.38, f32[256,512]{1,0:T(8,128)} %fusion.101, f32[2048]{0:T(1024)S(1)} %copy-done.7, f32[256]{0:T(256)S(1)} %add_rsqrt_fusion), kind=kOutput, calls=%fused_computation.17 | convolution fusion | flops 1078722560 | bytes 8922112 | tf_op jit(solution)/shard_map/dot_general | solution.py:300
  (24 shorter events, 0.1 us)
Async XLA Ops:
  0.0 155.7 %copy-start = (bf16[1,512,2048]{2,1,0:T(8,128)(2,1)S(1)}, bf16[1,512,2048]{2,1,0:T(8,128)(2,1)}, u32[]{:S(2)}) copy-start(bf16[1,512,2048]{2,1,0:T(8,128)(2,1)} %param.36) | copy-start | bytes 6291460
  0.0 28.4 %copy-start.8 = (s32[256,4]{0,1:T(4,128)S(1)}, s32[256,4]{0,1:T(4,128)}, u32[]{:S(2)}) copy-start(s32[256,4]{0,1:T(4,128)} %param.32) | copy-start | bytes 12292
  23.1 13.2 %all-to-all-start = ((f32[4,128,256]{2,1,0:T(8,128)}), f32[4,128,256]{2,1,0:T(8,128)S(1)}, u32[]{:S(2)}, u32[]{:S(2)}) async-start(f32[4,128,256]{2,1,0:T(8,128)} %get-tuple-element.14), calls=%async_computation | async-start | bytes 1048576 | tf_op jit(solution)/shard_map/all_to_all | solution.py:256
  36.3 0.8 copy-start.4
  71.6 8.9 %all-to-all-start.1 = ((f32[4,128,128]{2,1,0:T(8,128)}), f32[4,128,128]{2,1,0:T(8,128)S(1)}, u32[]{:S(2)}, u32[]{:S(2)}) async-start(f32[4,128,128]{2,1,0:T(8,128)} %states.1), calls=%async_computation.1 | async-start | bytes 524288 | tf_op jit(solution)/shard_map/all_to_all | solution.py:262
  80.5 0.7 copy-start.5
  85.5 15.1 %copy-start.6 = (bf16[256,2048]{1,0:T(8,128)(2,1)S(1)}, bf16[256,2048]{1,0:T(8,128)(2,1)}, u32[]{:S(2)}) copy-start(bf16[256,2048]{1,0:T(8,128)(2,1)} %param.30) | copy-start | bytes 3145732
  98.1 2.8 copy-start.2
  100.9 0.9 copy-start.7
  105.3 35.8 %all-to-all-start.5 = ((bf16[128,8,1024]{2,1,0:T(8,128)(2,1)}), bf16[128,8,1024]{2,1,0:T(8,128)(2,1)}, u32[]{:S(2)}, u32[]{:S(2)}) async-start(bf16[128,8,1024]{2,1,0:T(8,128)(2,1)} %fusion.23), calls=%async_computation.5 | async-start | bytes 4194304 | tf_op jit(solution)/shard_map/all_to_all | solution.py:304
  141.1 58.2 %all-to-all-start.3 = ((bf16[128,8,2048]{2,1,0:T(8,128)(2,1)}), bf16[128,8,2048]{2,1,0:T(8,128)(2,1)}, u32[]{:S(2)}, u32[]{:S(2)}) async-start(bf16[128,8,2048]{2,1,0:T(8,128)(2,1)} %convert_bitcast_fusion.1), calls=%async_computation.3 | async-start | bytes 8388608 | tf_op jit(solution)/shard_map/all_to_all | solution.py:304
  151.5 2.0 copy-start.10
  152.2 1.3 copy-start.3
  199.3 35.7 %all-to-all-start.6 = ((bf16[128,8,1024]{2,1,0:T(8,128)(2,1)}), bf16[128,8,1024]{2,1,0:T(8,128)(2,1)}, u32[]{:S(2)}, u32[]{:S(2)}) async-start(bf16[128,8,1024]{2,1,0:T(8,128)(2,1)} %reshape.251), calls=%async_computation.6 | async-start | bytes 4194304 | tf_op jit(solution)/shard_map/all_to_all | solution.py:304
  221.4 19.2 %copy-start.9 = (f32[256,4]{0,1:T(4,128)S(1)}, f32[256,4]{0,1:T(4,128)}, u32[]{:S(2)}) copy-start(f32[256,4]{0,1:T(4,128)} %param.33) | copy-start | bytes 12292
  235.0 58.2 %all-to-all-start.4 = ((bf16[128,8,2048]{2,1,0:T(8,128)(2,1)}), bf16[128,8,2048]{2,1,0:T(8,128)(2,1)}, u32[]{:S(2)}, u32[]{:S(2)}) async-start(bf16[128,8,2048]{2,1,0:T(8,128)(2,1)} %convert_bitcast_fusion), calls=%async_computation.4 | async-start | bytes 8388608 | tf_op jit(solution)/shard_map/all_to_all | solution.py:304
  298.5 5.6 %copy-start.1 = (bf16[1,512,2048]{2,1,0:T(8,128)(2,1)S(1)}, bf16[1,512,2048]{2,1,0:T(8,128)(2,1)}, u32[]{:S(2)}) copy-start(bf16[1,512,2048]{2,1,0:T(8,128)(2,1)} %param.36) | copy-start | bytes 6291460
